TPU v7x, 32 devices: a whole 2x2x4 slice. The times are simulated.
32 devices in a mesh: ep: 32 (over z, y, x, core).
Axes of the slice: x: 2, y: 2, z: 4, core: 2. Of those that a mesh axis runs over, the one named last changes fastest.
Arguments:
- tokens: bfloat16 [1024, 3072], P('ep'), may hold values from -6 to 6
- norm_gain: float32 [3072], replicated, may hold values from 0.1 to 1.9
- expert_ids: int32 [1024, 4], P('ep'), may hold values from 0 to 31, as said below
- expert_scores: float32 [1024, 4], P('ep'), may hold values from -100 to 180
- group_prob: float32 [1024], P('ep'), may hold values from 0.25 to 1
- gate_weight: bfloat16 [32, 3072, 384], P('ep'), may hold values from -0.109375 to 0.109375
- up_weight: bfloat16 [32, 3072, 384], P('ep'), may hold values from -0.109375 to 0.109375
- down_weight: bfloat16 [32, 384, 3072], P('ep'), may hold values from -0.3125 to 0.3125
Outputs:
- combined: bfloat16 [1024, 3072], P('ep')
Inputs may be any that keep to these rules, and one draw needn't show every extreme that they name: `expert_ids`: the 4 ids of a row are different and lie in one group of 8 consecutive experts. Among the rows of one device no expert is named by more than 16 rows, and in every draw some expert is named by exactly 16 rows of one device.
All inputs are finite; a program needn't handle non-finite values.
Results may differ from a plain program's by a relative error of at most 0.0085.
Values may be sent and summed in bfloat16 or wider, within the bound.
No kernel may reach another device: no remote copies, remote signals or barrier semaphores. Data moves between devices by JAX's collectives and lax.ppermute only.
A program may use at most 128 MiB of HBM per device.

v0:
```python
import jax
import jax.numpy as jnp
from jax import lax
from jax.sharding import PartitionSpec as P

GROUPS = 4
TOP_K = 4


eps_norm = 1e-05


def layer_norm(tokens, norm_gain):
    values = tokens.astype(jnp.float32)
    average = jnp.mean(values, axis=1, keepdims=True)
    centred = values - average
    variance = jnp.mean(centred * centred, axis=1, keepdims=True)
    return (centred * lax.rsqrt(variance + eps_norm) * norm_gain[None, :]).astype(jnp.bfloat16)


def mixing_weights(expert_scores, group_prob):
    shifted = expert_scores - jnp.max(expert_scores, axis=1, keepdims=True)
    exp_scores = jnp.exp(shifted)
    return exp_scores / jnp.sum(exp_scores, axis=1, keepdims=True) * group_prob[:, None]


def expert_rows(flat_rows, gate_matrix, up_matrix, down_matrix):
    gate_act = jnp.dot(flat_rows, gate_matrix, preferred_element_type=jnp.float32)
    up_act = jnp.dot(flat_rows, up_matrix, preferred_element_type=jnp.float32)
    hidden = (jax.nn.silu(gate_act) * up_act).astype(jnp.bfloat16)
    return jnp.dot(hidden, down_matrix, preferred_element_type=jnp.float32).astype(jnp.bfloat16)


def local(
    tokens, norm_gain, expert_ids, expert_scores, group_prob, gate_weight, up_weight, down_weight
):
    normed = layer_norm(tokens, norm_gain)
    weights_tok = mixing_weights(expert_scores, group_prob)
    tok_count = tokens.shape[0]
    model_width = tokens.shape[1]
    expert_count = lax.axis_size("ep")
    group_size = expert_count // GROUPS
    capacity = (tok_count * TOP_K + group_size - 1) // group_size
    expert_iota = jnp.arange(expert_count, dtype=jnp.int32)
    slot_iota = jnp.arange(capacity, dtype=jnp.int32)
    matches = expert_ids[:, :, None] == expert_iota[None, None, :]
    route_weight = jnp.sum(jnp.where(matches, weights_tok[:, :, None], 0.0), axis=1)
    gate_matrix = gate_weight[0]
    up_matrix = up_weight[0]
    down_matrix = down_weight[0]
    chosen = jnp.sum(matches.astype(jnp.int32), axis=1)
    order_rank = jnp.cumsum(chosen, axis=0) - chosen
    slot_map = (chosen.T[:, None, :] == 1) & (order_rank.T[:, None, :] == slot_iota[None, :, None])
    outgoing = jnp.einsum(
        "emt,td->emd", slot_map.astype(jnp.bfloat16), normed, preferred_element_type=jnp.float32
    ).astype(jnp.bfloat16)
    received = lax.all_to_all(outgoing, "ep", split_axis=0, concat_axis=0, tiled=True)
    flat_rows = received.reshape(-1, model_width)
    results = expert_rows(flat_rows, gate_matrix, up_matrix, down_matrix).reshape(received.shape)
    returned_rows = lax.all_to_all(results, "ep", split_axis=0, concat_axis=0, tiled=True)
    slot_scale = jnp.where(slot_map, route_weight.T[:, None, :], 0.0)
    mixture = jnp.einsum(
        "emt,emd->td",
        slot_scale,
        returned_rows.astype(jnp.float32),
        precision=lax.Precision.HIGHEST,
    )
    return mixture.astype(jnp.bfloat16)


def solution(mesh):
    in_specs = (
        P("ep", None),
        P(),
        P("ep", None),
        P("ep", None),
        P("ep"),
        P("ep", None, None),
        P("ep", None, None),
        P("ep", None, None),
    )
    out_specs = P("ep", None)
    return jax.shard_map(local, mesh=mesh, in_specs=in_specs, out_specs=out_specs, check_vma=False)
```

profile of v0, /device:TPU:0, one launch (start us, length us, event | category | flops | bytes accessed | tf_op | source)
XLA Modules:
  0.0 176.0 jit_solution(9429624024677687291)
XLA Ops:
  0.0 0.0 copy-start
  0.0 0.9 convert_reduce_fusion.1
  0.9 0.1 reduce_window_sum.11
  1.1 0.2 copy.17
  1.2 1.1 convert_reduce_fusion
  2.3 1.2 fusion.22
  3.5 2.0 %convolution_convert_fusion.1 = bf16[32,16,3072]{2,1,0:T(8,128)(2,1)S(1)} fusion(pred[32,16,32]{2,1,0:T(8,128)(4,1)S(1)} %copy.17, bf16[32,3072]{1,0:T(8,128)(2,1)} %param.8, f32[3072]{0:T(1024)} %param.9, f32[32]{0:T(128)S(1)} %add_rsqrt_fusion, f32[32]{0:T(128)S(1)} %broadcast_multiply_fusion), kind=kOutput, calls=%fused_computation.1 | convolution fusion | flops 102727680 | bytes 3371264 | tf_op jit(solution)/shard_map/emt,td->emd/dot_general | solution.py:54
  5.5 0.0 copy-start.5
  5.5 78.3 %all_to_all.10 = bf16[32,16,3072]{2,1,0:T(8,128)(2,1)S(1)} all-to-all(bf16[32,16,3072]{2,1,0:T(8,128)(2,1)S(1)} %convolution_convert_fusion.1), channel_id=1, replica_groups=mesh['ep'=32] {'ep'}, dimensions={0} | all-to-all | bytes 6291456 | tf_op jit(solution)/shard_map/all_to_all | solution.py:57
  83.7 0.0 copy-start.1
  83.7 1.7 copy-done.1
  85.4 0.0 copy-done.5
  85.4 1.8 %fusion.5 = f32[512,384]{1,0:T(8,128)S(1)} fusion(bf16[512,3072]{1,0:T(8,128)(2,1)S(1)} %bitcast.33, bf16[1,3072,384]{2,1,0:T(8,128)(2,1)S(1)} %copy-done.5), kind=kOutput, calls=%fused_computation.8 | convolution fusion | flops 1207959552 | bytes 6291456 | tf_op jit(solution)/shard_map/dot_general | solution.py:28
  87.2 0.0 copy-done
  87.2 7.7 %convolution_convert_fusion = bf16[512,3072]{1,0:T(8,128)(2,1)} fusion(bf16[1,384,3072]{2,1,0:T(8,128)(2,1)S(1)} %copy-done, bf16[512,3072]{1,0:T(8,128)(2,1)} %bitcast.34, bf16[1,3072,384]{2,1,0:T(8,128)(2,1)} %param.14, f32[512,384]{1,0:T(8,128)S(1)} %fusion.5), kind=kOutput, calls=%fused_computation | convolution fusion | flops 2418671616 | bytes 11796480 | tf_op jit(solution)/shard_map/dot_general | solution.py:31
  95.0 0.0 copy-start.2
  95.0 0.0 copy-start.3
  95.0 3.8 %all-to-all-start.1 = ((bf16[32,16,3072]{2,1,0:T(8,128)(2,1)}), bf16[32,16,3072]{2,1,0:T(8,128)(2,1)}, u32[]{:S(2)}, u32[]{:S(2)}) async-start(bf16[32,16,3072]{2,1,0:T(8,128)(2,1)} %bitcast.32), calls=%async_computation.1 | async-start | bytes 6291456 | tf_op jit(solution)/shard_map/all_to_all | solution.py:60
  98.8 0.0 copy-done.2
  98.8 0.0 copy-done.4
  98.9 0.0 copy-done.3
  98.9 0.1 select_reduce_fusion
  99.0 71.1 %all-to-all-done.1 = bf16[32,16,3072]{2,1,0:T(8,128)(2,1)} async-done(((bf16[32,16,3072]{2,1,0:T(8,128)(2,1)}), bf16[32,16,3072]{2,1,0:T(8,128)(2,1)}, u32[]{:S(2)}, u32[]{:S(2)}) %all-to-all-start.1) | async-done | bytes 3145760 | tf_op jit(solution)/shard_map/all_to_all | solution.py:60
  170.1 5.9 %fusion = bf16[32,3072]{1,0:T(8,128)(2,1)} fusion(bf16[32,16,3072]{2,1,0:T(8,128)(2,1)} %all-to-all-done.1, f32[32,32]{0,1:T(8,128)S(1)} %bitcast.35, s32[32,32]{0,1:T(8,128)S(1)} %subtract_bitcast_fusion, pred[32,32]{0,1:T(8,128)(4,1)S(1)} %compare_bitcast_fusion), kind=kOutput, calls=%fused_computation.3 | convolution fusion | flops 604127232 | bytes 3351552 | tf_op jit(solution)/shard_map/emt,emd->td/dot_general | solution.py:62
  (9 shorter events, 0.1 us)
Async XLA Ops:
  0.0 87.2 %copy-start = (bf16[1,384,3072]{2,1,0:T(8,128)(2,1)S(1)}, bf16[1,384,3072]{2,1,0:T(8,128)(2,1)}, u32[]{:S(2)}) copy-start(bf16[1,384,3072]{2,1,0:T(8,128)(2,1)} %param.15) | copy-start | bytes 7077892
  5.5 80.0 %copy-start.5 = (bf16[1,3072,384]{2,1,0:T(8,128)(2,1)S(1)}, bf16[1,3072,384]{2,1,0:T(8,128)(2,1)}, u32[]{:S(2)}) copy-start(bf16[1,3072,384]{2,1,0:T(8,128)(2,1)} %param.13) | copy-start | bytes 7077892
  83.7 1.7 copy-start.1
  95.0 3.8 %copy-start.2 = (f32[32,4]{0,1:T(4,128)S(1)}, f32[32,4]{0,1:T(4,128)}, u32[]{:S(2)}) copy-start(f32[32,4]{0,1:T(4,128)} %param.11) | copy-start | bytes 1540
  95.0 3.8 %copy-start.4 = (f32[32]{0:T(128)S(1)}, f32[32]{0:T(128)}, u32[]{:S(2)}) copy-start(f32[32]{0:T(128)} %param.12) | copy-start | bytes 388
  95.0 3.9 %copy-start.3 = (s32[32,4]{0,1:T(4,128)S(1)}, s32[32,4]{0,1:T(4,128)}, u32[]{:S(2)}) copy-start(s32[32,4]{0,1:T(4,128)} %param.10) | copy-start | bytes 1540
  95.0 75.1 %all-to-all-start.1 = ((bf16[32,16,3072]{2,1,0:T(8,128)(2,1)}), bf16[32,16,3072]{2,1,0:T(8,128)(2,1)}, u32[]{:S(2)}, u32[]{:S(2)}) async-start(bf16[32,16,3072]{2,1,0:T(8,128)(2,1)} %bitcast.32), calls=%async_computation.1 | async-start | bytes 6291456 | tf_op jit(solution)/shard_map/all_to_all | solution.py:60
where the time goes:
time: 176 us
  blocking collectives  78.3 us (44%)
  waiting for transfers between devices  71.1 us (40%)
  matrix products  17.4 us (10%)
  starting transfers between devices  3.77 us (2%)
  other arithmetic  3.42 us (2%)
  local copies, waits for them, and re-layouts  1.91 us (1%)
    all_to_all x1, blocking collectives, local(): lax.all_to_all(outgoing, 'ep', split_axis=0, concat_axis=0, tiled=True)  78.3 us
    all_to_all x1, waiting for transfers between devices, local(): lax.all_to_all(results, 'ep', split_axis=0, concat_axis=0, tiled=True)  71.1 us
    dot_general x1, matrix products, expert_rows(): jnp.dot(hidden, down_matrix, preferred_element_type=jnp.float32)  7.74 us
    dot_general x1, matrix products, local(): jnp.einsum('emt,emd->td', slot_scale, returned_rows.astype(jnp.float32),...  5.89 us
    all_to_all x1, starting transfers between devices, local(): lax.all_to_all(results, 'ep', split_axis=0, concat_axis=0, tiled=True)  3.77 us
  transfers between devices with their start and end apart: 1, of which 1 were waited for; matrix products, arithmetic and copies ran while one was open for 0% of the time, Pallas kernels for 0%

commit v1 on v0

v1 whole, which is shorter than its diff:
```python
import functools

import jax
import jax.numpy as jnp
from jax import lax
from jax.experimental import pallas as pl
from jax.experimental.pallas import tpu as pltpu
from jax.sharding import PartitionSpec as P

GROUPS = 4
eps_norm = 1e-05

VMEM = pl.BlockSpec(memory_space=pltpu.VMEM)
f32 = jnp.float32
bf16 = jnp.bfloat16


def prepare_kernel(n, tokens_ref, gain_ref, ids_ref, scores_ref, prob_ref, out_ref, turn_ref):
    t, d = tokens_ref.shape
    k = ids_ref.shape[0]
    values = tokens_ref[...].astype(f32)
    average = jnp.mean(values, axis=1, keepdims=True)
    centred = values - average
    variance = jnp.mean(centred * centred, axis=1, keepdims=True)
    normed = centred * lax.rsqrt(variance + eps_norm) * gain_ref[...]
    out_ref[:, :d] = normed.astype(bf16)
    scores = scores_ref[...]
    exp_scores = jnp.exp(scores - jnp.max(scores, axis=0, keepdims=True))
    turn_ref[...] = jnp.zeros(turn_ref.shape, f32)
    turn_ref[:k, :t] = exp_scores / jnp.sum(exp_scores, axis=0, keepdims=True) * prob_ref[...]
    turn_ref[k : 2 * k, :t] = ids_ref[...].astype(f32)
    turned = turn_ref[...].T[:t]
    column = lax.broadcasted_iota(jnp.int32, (t, out_ref.shape[1] - d), 1)
    expert = jnp.where(column >= n, column - n, column).astype(f32)
    value = jnp.zeros(column.shape, f32)
    for j in range(k):
        value = value + jnp.where(expert == turned[:, k + j : k + j + 1], turned[:, j : j + 1], 0.0)
    high = value.astype(bf16).astype(f32)
    low = jnp.where(column < 2 * n, value - high, 0.0)
    out_ref[:, d:] = jnp.where(column < n, high, low).astype(bf16)


def prepare(tokens, norm_gain, expert_ids, expert_scores, group_prob, n):
    t, d = tokens.shape
    width = d + 2 * n + (-2 * n) % 128
    return pl.pallas_call(
        functools.partial(prepare_kernel, n),
        out_shape=jax.ShapeDtypeStruct((t, width), bf16),
        in_specs=[VMEM] * 5,
        out_specs=VMEM,
        scratch_shapes=[pltpu.VMEM((8, 128), f32)],
        compiler_params=pltpu.CompilerParams(vmem_limit_bytes=4 * 2**20),
        name="prepare",
    )(tokens, norm_gain[None, :], expert_ids.T, expert_scores.T, group_prob[None, :])


def expert_kernel(own_ref, other_ref, gate_ref, up_ref, down_ref, pick_ref, keep_ref, give_ref, x_ref, h_ref):
    m = own_ref.shape[0]
    d = keep_ref.shape[1]
    x_ref[:m] = own_ref[...]
    x_ref[m:] = other_ref[...]
    weight = jnp.sum(x_ref[:, d:].astype(f32) * pick_ref[...], axis=1, keepdims=True)
    x = x_ref[:, :d]
    gate = jnp.dot(x, gate_ref[0], preferred_element_type=f32)
    up = jnp.dot(x, up_ref[0], preferred_element_type=f32)
    h_ref[...] = (gate * jax.nn.sigmoid(gate) * up).astype(bf16)
    step = 256
    for j in range(0, d, step):
        out = jnp.dot(h_ref[...], down_ref[0, :, j : j + step], preferred_element_type=f32) * weight
        keep_ref[:, j : j + step] = out[:m]
        give_ref[:, j : j + step] = out[m:].astype(bf16)


def expert(own, other, gate_weight, up_weight, down_weight, pick):
    m, width = own.shape
    d, ffe = gate_weight.shape[1:]
    block = min(m, 128)
    weights = pl.BlockSpec(memory_space=pltpu.VMEM)
    rows = pl.BlockSpec((block, width), lambda i: (i, 0))
    outs = pl.BlockSpec((block, d), lambda i: (i, 0))
    single = m == block
    return pl.pallas_call(
        expert_kernel,
        grid=() if single else (m // block,),
        out_shape=(jax.ShapeDtypeStruct((m, d), f32), jax.ShapeDtypeStruct((m, d), bf16)),
        in_specs=[VMEM if single else rows] * 2 + [weights] * 4,
        out_specs=(VMEM, VMEM) if single else (outs, outs),
        scratch_shapes=[pltpu.VMEM((2 * block, width), bf16), pltpu.VMEM((2 * block, ffe), bf16)],
        compiler_params=pltpu.CompilerParams(vmem_limit_bytes=16 * 2**20),
        cost_estimate=pl.CostEstimate(
            flops=12 * m * d * ffe, bytes_accessed=20 * m * d, transcendentals=2 * m * ffe
        ),
        name="expert",
    )(own, other, gate_weight, up_weight, down_weight, pick)


def fold_kernel(keep_ref, got_ref, kept_ref, give_ref):
    half = kept_ref.shape[0]
    kept_ref[...] = keep_ref[:half] + got_ref[:half].astype(f32)
    give_ref[...] = (keep_ref[half:] + got_ref[half:].astype(f32)).astype(bf16)


def fold(keep, got):
    m, d = keep.shape
    block = min(m // 2, 128)
    if block * 2 == m:
        return pl.pallas_call(
            fold_kernel,
            out_shape=(
                jax.ShapeDtypeStruct((m // 2, d), f32),
                jax.ShapeDtypeStruct((m // 2, d), bf16),
            ),
            in_specs=[VMEM, VMEM],
            out_specs=(VMEM, VMEM),
            compiler_params=pltpu.CompilerParams(vmem_limit_bytes=4 * 2**20),
            cost_estimate=pl.CostEstimate(flops=m * d * 64, bytes_accessed=12 * m * d, transcendentals=0),
            name="fold",
        )(keep, got)
    total = keep + got.astype(f32)
    return total[: m // 2], total[m // 2 :].astype(bf16)


def local(
    tokens, norm_gain, expert_ids, expert_scores, group_prob, gate_weight, up_weight, down_weight
):
    n = lax.axis_size("ep")
    size = n // GROUPS
    _, d = tokens.shape
    bits = [1 << b for b in range(1, size.bit_length() - 1)]
    me = lax.axis_index("ep")

    def exchange(x, flip):
        return lax.ppermute(x, "ep", [(i, i ^ flip(i)) for i in range(n)])

    def plane(step):
        return lambda i: bits[step] if i % 2 == 0 else bits[-1 - step]

    def group(q):
        return lambda i: q * size

    sent = prepare(tokens, norm_gain, expert_ids, expert_scores, group_prob, n)
    columns = jnp.arange(sent.shape[1] - d)[None, :]
    pick = ((columns == me) | (columns == n + me)).astype(f32)
    shard = [sent, exchange(sent, group(1)), exchange(sent, group(2)), None]
    shard[3] = exchange(shard[2], group(1))
    parts = []
    for q in range(GROUPS):
        x = shard[q]
        for s in range(len(bits)):
            x = jnp.concatenate([x, exchange(x, plane(s))], axis=0)
        other = exchange(x, lambda i: 1)
        keep, give = expert(x, other, gate_weight, up_weight, down_weight, pick)
        got = exchange(give, lambda i: 1)
        for s in reversed(range(len(bits))):
            keep, give = fold(keep, got)
            got = exchange(give, plane(s))
        part = keep + got.astype(f32)
        if q:
            part = exchange(part.astype(bf16), group(q)).astype(f32)
        parts.append(part)
    return (parts[0] + parts[1] + parts[2] + parts[3]).astype(bf16)


def solution(mesh):
    in_specs = (
        P("ep", None), P(), P("ep", None), P("ep", None), P("ep"),
        P("ep", None, None), P("ep", None, None), P("ep", None, None),
    )

    return jax.shard_map(local, mesh=mesh, in_specs=in_specs, out_specs=P("ep", None), check_vma=False)
```

time: 176 us -> 99.1 us (0.56)
  blocking collectives: 78.3 us -> 0 us
  starting transfers between devices: 3.77 us -> 36.4 us
  waiting for transfers between devices: 71.1 us -> 45 us
  matrix products: 17.4 us -> 0 us
  Pallas kernels: 0 us -> 12.2 us
  other arithmetic: 3.42 us -> 1.13 us
  local copies, waits for them, and re-layouts: 1.91 us -> 3.88 us
    all_to_all x1 -> x0, blocking collectives: 78.3 us -> none  [local(): lax.all_to_all(outgoing, 'ep', split_axis=0, concat_axis=0, tiled=True)]
    all_to_all x1 -> x0, waiting for transfers between devices: 71.1 us -> none  [local(): lax.all_to_all(results, 'ep', split_axis=0, concat_axis=0, tiled=True)]
    ppermute x0 -> x30, waiting for transfers between devices: none -> 45 us  [exchange(): return lax.ppermute(x, 'ep', [(i, i ^ flip(i)) for i in range(n)])]
    ppermute x0 -> x30, starting transfers between devices: none -> 36.4 us  [exchange(): return lax.ppermute(x, 'ep', [(i, i ^ flip(i)) for i in range(n)])]
    dot_general x4 -> x0, matrix products: 17.4 us -> none  [the longest x1 7.74 us: expert_rows(): jnp.dot(hidden, down_matrix, preferred_element_type=jnp.float32)]
    pallas_call x0 -> x13, Pallas kernels: none -> 12.2 us  [the longest x4 11 us: expert(): pl.pallas_call(expert_kernel, grid=() if single else (m // block,), out_s...]
    all_to_all x1 -> x0, starting transfers between devices: 3.77 us -> none  [local(): lax.all_to_all(results, 'ep', split_axis=0, concat_axis=0, tiled=True)]
    reduce_sum x5 -> x0, other arithmetic: 3.26 us -> none  [the longest x1 1.16 us: layer_norm(): variance = jnp.mean(centred * centred, axis=1, keepdims=True)]
  transfers between devices with their start and end apart: 1 -> 30, of which waited for: 1 -> 13; matrix products, arithmetic and copies ran while one was open for 0% -> 1% of each run, Pallas kernels for 0% -> 12%
where the time goes in v1:
time: 99.1 us; the launch traced here: 98.8 us
  waiting for transfers between devices  45 us (45%)
  starting transfers between devices  36.4 us (37%)
  Pallas kernels  12.2 us (12%)
  local copies, waits for them, and re-layouts  3.88 us (4%)
  other arithmetic  1.13 us (1%)
    ppermute x30, waiting for transfers between devices, exchange(): return lax.ppermute(x, 'ep', [(i, i ^ flip(i)) for i in range(n)])  45 us
    ppermute x30, starting transfers between devices, exchange(): return lax.ppermute(x, 'ep', [(i, i ^ flip(i)) for i in range(n)])  36.4 us
    pallas_call x4, Pallas kernels, expert(): pl.pallas_call(expert_kernel, grid=() if single else (m // block,), out_s...  11 us
    unnamed x22, local copies, waits for them, and re-layouts  3.77 us
  transfers between devices with their start and end apart: 30, of which 13 were waited for; matrix products, arithmetic and copies ran while one was open for 1% of the time, Pallas kernels for 12%

profile of v1, /device:TPU:0, one launch (start us, length us, event | category | flops | bytes accessed | tf_op | source)
XLA Modules:
  0.0 98.8 jit_solution(8429760870505803437)
XLA Ops:
  4.0 3.0 %collective-permute-start = (bf16[32,3200]{1,0:T(8,128)(2,1)S(1)}, bf16[32,3200]{1,0:T(8,128)(2,1)S(1)}, u32[]{:S(2)}, u32[]{:S(2)}) collective-permute-start(bf16[32,3200]{1,0:T(8,128)(2,1)S(1)} %prepare.1), channel_id=1, source_target_pairs={{0,2},{1,5},{2,0},{3,7},{4,6},{5,1},{6,4},{7,3},{8,10},{9,13},{10,... | collective-permute-start | bytes 614408 | tf_op jit(solution)/shard_map/ppermute | solution.py:133
  7.0 2.6 %collective-permute-start.14 = (bf16[32,3200]{1,0:T(8,128)(2,1)S(1)}, bf16[32,3200]{1,0:T(8,128)(2,1)S(1)}, u32[]{:S(2)}, u32[]{:S(2)}) collective-permute-start(bf16[32,3200]{1,0:T(8,128)(2,1)S(1)} %prepare.1), channel_id=1, source_target_pairs={{0,16},{1,17},{2,18},{3,19},{4,20},{5,21},{6,22},{7,23},{8,24},{9,... | collective-permute-start | bytes 614408 | tf_op jit(solution)/shard_map/ppermute | solution.py:133
  9.6 1.6 %collective-permute-start.6 = (bf16[32,3200]{1,0:T(8,128)(2,1)S(1)}, bf16[32,3200]{1,0:T(8,128)(2,1)S(1)}, u32[]{:S(2)}, u32[]{:S(2)}) collective-permute-start(bf16[32,3200]{1,0:T(8,128)(2,1)S(1)} %prepare.1), channel_id=1, source_target_pairs={{0,8},{1,9},{2,10},{3,11},{4,12},{5,13},{6,14},{7,15},{8,0},{9,1},... | collective-permute-start | bytes 614408 | tf_op jit(solution)/shard_map/ppermute | solution.py:133
  11.2 1.7 %collective-permute-start.1 = (bf16[64,3200]{1,0:T(8,128)(2,1)S(1)}, bf16[64,3200]{1,0:T(8,128)(2,1)S(1)}, u32[]{:S(2)}, u32[]{:S(2)}) collective-permute-start(bf16[64,3200]{1,0:T(8,128)(2,1)S(1)} %pad_maximum_fusion.1), channel_id=1, source_target_pairs={{0,4},{1,3},{2,6},{3,1},{4,0},{5,7},{6,2},{7,5},{8,12},{9,11},{10,... | collective-permute-start | bytes 1228808 | tf_op jit(solution)/shard_map/ppermute | solution.py:133
  12.9 6.1 %collective-permute-done.14 = bf16[32,3200]{1,0:T(8,128)(2,1)S(1)} collective-permute-done((bf16[32,3200]{1,0:T(8,128)(2,1)S(1)}, bf16[32,3200]{1,0:T(8,128)(2,1)S(1)}, u32[]{:S(2)}, u32[]{:S(2)}) %collective-permute-start.14) | collective-permute-done | bytes 204832 | tf_op jit(solution)/shard_map/ppermute | solution.py:133
  19.6 1.6 %collective-permute-start.15 = (bf16[32,3200]{1,0:T(8,128)(2,1)S(1)}, bf16[32,3200]{1,0:T(8,128)(2,1)S(1)}, u32[]{:S(2)}, u32[]{:S(2)}) collective-permute-start(bf16[32,3200]{1,0:T(8,128)(2,1)S(1)} %collective-permute-done.14), channel_id=1, source_target_pairs={{0,2},{1,5},{2,0},{3,7},{4,6},{5,1},{6,4},{7,3},{8,10},{9,13},{10,... | collective-permute-start | bytes 614408 | tf_op jit(solution)/shard_map/ppermute | solution.py:133
  21.8 3.6 %collective-permute-done.15 = bf16[32,3200]{1,0:T(8,128)(2,1)S(1)} collective-permute-done((bf16[32,3200]{1,0:T(8,128)(2,1)S(1)}, bf16[32,3200]{1,0:T(8,128)(2,1)S(1)}, u32[]{:S(2)}, u32[]{:S(2)}) %collective-permute-start.15) | collective-permute-done | bytes 204832 | tf_op jit(solution)/shard_map/ppermute | solution.py:133
  26.0 2.2 %collective-permute-done.7 = bf16[32,3200]{1,0:T(8,128)(2,1)S(1)} collective-permute-done((bf16[32,3200]{1,0:T(8,128)(2,1)S(1)}, bf16[32,3200]{1,0:T(8,128)(2,1)S(1)}, u32[]{:S(2)}, u32[]{:S(2)}) %collective-permute-start.7) | collective-permute-done | bytes 204832 | tf_op jit(solution)/shard_map/ppermute | solution.py:133
  30.5 6.6 %collective-permute-done.23 = bf16[32,3200]{1,0:T(8,128)(2,1)S(1)} collective-permute-done((bf16[32,3200]{1,0:T(8,128)(2,1)S(1)}, bf16[32,3200]{1,0:T(8,128)(2,1)S(1)}, u32[]{:S(2)}, u32[]{:S(2)}) %collective-permute-start.23) | collective-permute-done | bytes 204832 | tf_op jit(solution)/shard_map/ppermute | solution.py:133
  40.2 4.9 %collective-permute-done.24 = bf16[64,3200]{1,0:T(8,128)(2,1)S(1)} collective-permute-done((bf16[64,3200]{1,0:T(8,128)(2,1)S(1)}, bf16[64,3200]{1,0:T(8,128)(2,1)S(1)}, u32[]{:S(2)}, u32[]{:S(2)}) %collective-permute-start.24) | collective-permute-done | bytes 409632 | tf_op jit(solution)/shard_map/ppermute | solution.py:133
  45.3 2.7 %expert.6 = (f32[128,3072]{1,0:T(8,128)S(1)}, bf16[128,3072]{1,0:T(8,128)(2,1)S(1)}) custom-call(bf16[128,3200]{1,0:T(8,128)(2,1)S(1)} %constant_dynamic-update-slice_fusion.3.own_ref, bf16[128,3200]{1,0:T(8,128)(2,1)S(1)} %collective-permute-done.17.other_ref, bf16[1,3072,384]{2,1,0:T(8,128)(2,1)S(1)} %copy-done, bf16[1,3072,384]{2,1,0:T(8,128)(2,1)S(1)} %copy-done.1, ...), custom_call_target="tpu_custom_call" | custom-call | flops 1811939328 | bytes 7864320 | tf_op jit(solution)/shard_map/expert/pallas_call | solution.py:82
  48.5 2.8 %expert.4 = (f32[128,3072]{1,0:T(8,128)S(1)}, bf16[128,3072]{1,0:T(8,128)(2,1)S(1)}) custom-call(bf16[128,3200]{1,0:T(8,128)(2,1)S(1)} %pad_maximum_fusion.own_ref, bf16[128,3200]{1,0:T(8,128)(2,1)S(1)} %collective-permute-done.2.other_ref, bf16[1,3072,384]{2,1,0:T(8,128)(2,1)S(1)} %copy-done, bf16[1,3072,384]{2,1,0:T(8,128)(2,1)S(1)} %copy-done.1, ...), custom_call_target="tpu_custom_call" | custom-call | flops 1811939328 | bytes 7864320 | tf_op jit(solution)/shard_map/expert/pallas_call | solution.py:82
  51.4 2.7 %expert.5 = (f32[128,3072]{1,0:T(8,128)S(1)}, bf16[128,3072]{1,0:T(8,128)(2,1)S(1)}) custom-call(bf16[128,3200]{1,0:T(8,128)(2,1)S(1)} %constant_dynamic-update-slice_fusion.own_ref, bf16[128,3200]{1,0:T(8,128)(2,1)S(1)} %collective-permute-done.9.other_ref, bf16[1,3072,384]{2,1,0:T(8,128)(2,1)S(1)} %copy-done, bf16[1,3072,384]{2,1,0:T(8,128)(2,1)S(1)} %copy-done.1, ...), custom_call_target="tpu_custom_call" | custom-call | flops 1811939328 | bytes 7864320 | tf_op jit(solution)/shard_map/expert/pallas_call | solution.py:82
  54.7 2.7 %expert.7 = (f32[128,3072]{1,0:T(8,128)S(1)}, bf16[128,3072]{1,0:T(8,128)(2,1)S(1)}) custom-call(bf16[128,3200]{1,0:T(8,128)(2,1)S(1)} %constant_dynamic-update-slice_fusion.6.own_ref, bf16[128,3200]{1,0:T(8,128)(2,1)S(1)} %collective-permute-done.25.other_ref, bf16[1,3072,384]{2,1,0:T(8,128)(2,1)S(1)} %copy-done, bf16[1,3072,384]{2,1,0:T(8,128)(2,1)S(1)} %copy-done.1, ...), custom_call_target="tpu_custom_call" | custom-call | flops 1811939328 | bytes 7864320 | tf_op jit(solution)/shard_map/expert/pallas_call | solution.py:82
  61.6 3.9 %collective-permute-done.19.got_ref = bf16[64,3072]{1,0:T(8,128)(2,1)S(1)} collective-permute-done((bf16[64,3072]{1,0:T(8,128)(2,1)S(1)}, bf16[64,3072]{1,0:T(8,128)(2,1)S(1)}, u32[]{:S(2)}, u32[]{:S(2)}) %collective-permute-start.19) | collective-permute-done | bytes 393248 | tf_op jit(solution)/shard_map/ppermute | solution.py:133
  67.0 4.6 %collective-permute-done.4.got_ref = bf16[64,3072]{1,0:T(8,128)(2,1)S(1)} collective-permute-done((bf16[64,3072]{1,0:T(8,128)(2,1)S(1)}, bf16[64,3072]{1,0:T(8,128)(2,1)S(1)}, u32[]{:S(2)}, u32[]{:S(2)}) %collective-permute-start.4) | collective-permute-done | bytes 393248 | tf_op jit(solution)/shard_map/ppermute | solution.py:133
  73.3 1.6 %collective-permute-start.27 = (bf16[64,3072]{1,0:T(8,128)(2,1)S(1)}, bf16[64,3072]{1,0:T(8,128)(2,1)S(1)}, u32[]{:S(2)}, u32[]{:S(2)}) collective-permute-start(bf16[64,3072]{1,0:T(8,128)(2,1)S(1)} %get-tuple-element.50), channel_id=1, source_target_pairs={{0,4},{1,3},{2,6},{3,1},{4,0},{5,7},{6,2},{7,5},{8,12},{9,11},{10,... | collective-permute-start | bytes 1179656 | tf_op jit(solution)/shard_map/ppermute | solution.py:133
  74.9 3.3 %collective-permute-done.11.got_ref = bf16[64,3072]{1,0:T(8,128)(2,1)S(1)} collective-permute-done((bf16[64,3072]{1,0:T(8,128)(2,1)S(1)}, bf16[64,3072]{1,0:T(8,128)(2,1)S(1)}, u32[]{:S(2)}, u32[]{:S(2)}) %collective-permute-start.11) | collective-permute-done | bytes 393248 | tf_op jit(solution)/shard_map/ppermute | solution.py:133
  79.7 3.4 %collective-permute-start.21 = (bf16[32,3072]{1,0:T(8,128)(2,1)S(1)}, bf16[32,3072]{1,0:T(8,128)(2,1)S(1)}, u32[]{:S(2)}, u32[]{:S(2)}) collective-permute-start(bf16[32,3072]{1,0:T(8,128)(2,1)S(1)} %add_convert_fusion.2), channel_id=1, source_target_pairs={{0,16},{1,17},{2,18},{3,19},{4,20},{5,21},{6,22},{7,23},{8,24},{9,... | collective-permute-start | bytes 589832 | tf_op jit(solution)/shard_map/ppermute | solution.py:133
  86.0 1.8 %collective-permute-start.13 = (bf16[32,3072]{1,0:T(8,128)(2,1)S(1)}, bf16[32,3072]{1,0:T(8,128)(2,1)S(1)}, u32[]{:S(2)}, u32[]{:S(2)}) collective-permute-start(bf16[32,3072]{1,0:T(8,128)(2,1)S(1)} %add_convert_fusion.3), channel_id=1, source_target_pairs={{0,8},{1,9},{2,10},{3,11},{4,12},{5,13},{6,14},{7,15},{8,0},{9,1},... | collective-permute-start | bytes 589832 | tf_op jit(solution)/shard_map/ppermute | solution.py:133
  87.8 2.5 %collective-permute-done.28 = bf16[32,3072]{1,0:T(8,128)(2,1)S(1)} collective-permute-done((bf16[32,3072]{1,0:T(8,128)(2,1)S(1)}, bf16[32,3072]{1,0:T(8,128)(2,1)S(1)}, u32[]{:S(2)}, u32[]{:S(2)}) %collective-permute-start.28) | collective-permute-done | bytes 196640 | tf_op jit(solution)/shard_map/ppermute | solution.py:133
  90.4 2.6 %collective-permute-start.29 = (bf16[32,3072]{1,0:T(8,128)(2,1)S(1)}, bf16[32,3072]{1,0:T(8,128)(2,1)S(1)}, u32[]{:S(2)}, u32[]{:S(2)}) collective-permute-start(bf16[32,3072]{1,0:T(8,128)(2,1)S(1)} %add_convert_fusion.1), channel_id=1, source_target_pairs={{0,24},{1,25},{2,26},{3,27},{4,28},{5,29},{6,30},{7,31},{8,16},{9,... | collective-permute-start | bytes 589832 | tf_op jit(solution)/shard_map/ppermute | solution.py:133
  93.0 1.5 %collective-permute-done.13 = bf16[32,3072]{1,0:T(8,128)(2,1)S(1)} collective-permute-done((bf16[32,3072]{1,0:T(8,128)(2,1)S(1)}, bf16[32,3072]{1,0:T(8,128)(2,1)S(1)}, u32[]{:S(2)}, u32[]{:S(2)}) %collective-permute-start.13) | collective-permute-done | bytes 196640 | tf_op jit(solution)/shard_map/ppermute | solution.py:133
  94.5 3.5 %collective-permute-done.29 = bf16[32,3072]{1,0:T(8,128)(2,1)S(1)} collective-permute-done((bf16[32,3072]{1,0:T(8,128)(2,1)S(1)}, bf16[32,3072]{1,0:T(8,128)(2,1)S(1)}, u32[]{:S(2)}, u32[]{:S(2)}) %collective-permute-start.29) | collective-permute-done | bytes 196640 | tf_op jit(solution)/shard_map/ppermute | solution.py:133
  (84 shorter events, 24.9 us)
Async XLA Ops:
  7.0 12.0 %collective-permute-start.14 = (bf16[32,3200]{1,0:T(8,128)(2,1)S(1)}, bf16[32,3200]{1,0:T(8,128)(2,1)S(1)}, u32[]{:S(2)}, u32[]{:S(2)}) collective-permute-start(bf16[32,3200]{1,0:T(8,128)(2,1)S(1)} %prepare.1), channel_id=1, source_target_pairs={{0,16},{1,17},{2,18},{3,19},{4,20},{5,21},{6,22},{7,23},{8,24},{9,... | collective-permute-start | bytes 614408 | tf_op jit(solution)/shard_map/ppermute | solution.py:133
  9.6 11.5 %collective-permute-start.6 = (bf16[32,3200]{1,0:T(8,128)(2,1)S(1)}, bf16[32,3200]{1,0:T(8,128)(2,1)S(1)}, u32[]{:S(2)}, u32[]{:S(2)}) collective-permute-start(bf16[32,3200]{1,0:T(8,128)(2,1)S(1)} %prepare.1), channel_id=1, source_target_pairs={{0,8},{1,9},{2,10},{3,11},{4,12},{5,13},{6,14},{7,15},{8,0},{9,1},... | collective-permute-start | bytes 614408 | tf_op jit(solution)/shard_map/ppermute | solution.py:133
  11.2 27.2 %collective-permute-start.1 = (bf16[64,3200]{1,0:T(8,128)(2,1)S(1)}, bf16[64,3200]{1,0:T(8,128)(2,1)S(1)}, u32[]{:S(2)}, u32[]{:S(2)}) collective-permute-start(bf16[64,3200]{1,0:T(8,128)(2,1)S(1)} %pad_maximum_fusion.1), channel_id=1, source_target_pairs={{0,4},{1,3},{2,6},{3,1},{4,0},{5,7},{6,2},{7,5},{8,12},{9,11},{10,... | collective-permute-start | bytes 1228808 | tf_op jit(solution)/shard_map/ppermute | solution.py:133
  19.0 10.0 %collective-permute-start.22 = (bf16[32,3200]{1,0:T(8,128)(2,1)S(1)}, bf16[32,3200]{1,0:T(8,128)(2,1)S(1)}, u32[]{:S(2)}, u32[]{:S(2)}) collective-permute-start(bf16[32,3200]{1,0:T(8,128)(2,1)S(1)} %collective-permute-done.14), channel_id=1, source_target_pairs={{0,8},{1,9},{2,10},{3,11},{4,12},{5,13},{6,14},{7,15},{8,0},{9,1},... | collective-permute-start | bytes 614408 | tf_op jit(solution)/shard_map/ppermute | solution.py:133
  25.4 13.2 %collective-permute-start.16 = (bf16[64,3200]{1,0:T(8,128)(2,1)S(1)}, bf16[64,3200]{1,0:T(8,128)(2,1)S(1)}, u32[]{:S(2)}, u32[]{:S(2)}) collective-permute-start(bf16[64,3200]{1,0:T(8,128)(2,1)S(1)} %pad_maximum_fusion.3), channel_id=1, source_target_pairs={{0,4},{1,3},{2,6},{3,1},{4,0},{5,7},{6,2},{7,5},{8,12},{9,11},{10,... | collective-permute-start | bytes 1228808 | tf_op jit(solution)/shard_map/ppermute | solution.py:133
  28.3 11.8 %collective-permute-start.8 = (bf16[64,3200]{1,0:T(8,128)(2,1)S(1)}, bf16[64,3200]{1,0:T(8,128)(2,1)S(1)}, u32[]{:S(2)}, u32[]{:S(2)}) collective-permute-start(bf16[64,3200]{1,0:T(8,128)(2,1)S(1)} %pad_maximum_fusion.2), channel_id=1, source_target_pairs={{0,4},{1,3},{2,6},{3,1},{4,0},{5,7},{6,2},{7,5},{8,12},{9,11},{10,... | collective-permute-start | bytes 1228808 | tf_op jit(solution)/shard_map/ppermute | solution.py:133
  29.0 8.0 %collective-permute-start.23 = (bf16[32,3200]{1,0:T(8,128)(2,1)S(1)}, bf16[32,3200]{1,0:T(8,128)(2,1)S(1)}, u32[]{:S(2)}, u32[]{:S(2)}) collective-permute-start(bf16[32,3200]{1,0:T(8,128)(2,1)S(1)} %collective-permute-done.22), channel_id=1, source_target_pairs={{0,2},{1,5},{2,0},{3,7},{4,6},{5,1},{6,4},{7,3},{8,10},{9,13},{10,... | collective-permute-start | bytes 614408 | tf_op jit(solution)/shard_map/ppermute | solution.py:133
  37.1 8.0 %collective-permute-start.24 = (bf16[64,3200]{1,0:T(8,128)(2,1)S(1)}, bf16[64,3200]{1,0:T(8,128)(2,1)S(1)}, u32[]{:S(2)}, u32[]{:S(2)}) collective-permute-start(bf16[64,3200]{1,0:T(8,128)(2,1)S(1)} %pad_maximum_fusion.4), channel_id=1, source_target_pairs={{0,4},{1,3},{2,6},{3,1},{4,0},{5,7},{6,2},{7,5},{8,12},{9,11},{10,... | collective-permute-start | bytes 1228808 | tf_op jit(solution)/shard_map/ppermute | solution.py:133
  38.6 10.0 %collective-permute-start.2 = (bf16[128,3200]{1,0:T(8,128)(2,1)S(1)}, bf16[128,3200]{1,0:T(8,128)(2,1)S(1)}, u32[]{:S(2)}, u32[]{:S(2)}) collective-permute-start(bf16[128,3200]{1,0:T(8,128)(2,1)S(1)} %pad_maximum_fusion.own_ref), channel_id=1, source_target_pairs={{0,1},{1,0},{2,3},{3,2},{4,5},{5,4},{6,7},{7,6},{8,9},{9,8},{10,11... | collective-permute-start | bytes 2457608 | tf_op jit(solution)/shard_map/ppermute | solution.py:133
  40.1 11.3 %collective-permute-start.9 = (bf16[128,3200]{1,0:T(8,128)(2,1)S(1)}, bf16[128,3200]{1,0:T(8,128)(2,1)S(1)}, u32[]{:S(2)}, u32[]{:S(2)}) collective-permute-start(bf16[128,3200]{1,0:T(8,128)(2,1)S(1)} %constant_dynamic-update-slice_fusion.own_ref), channel_id=1, source_target_pairs={{0,1},{1,0},{2,3},{3,2},{4,5},{5,4},{6,7},{7,6},{8,9},{9,8},{10,11... | collective-permute-start | bytes 2457608 | tf_op jit(solution)/shard_map/ppermute | solution.py:133
  45.1 9.6 %collective-permute-start.25 = (bf16[128,3200]{1,0:T(8,128)(2,1)S(1)}, bf16[128,3200]{1,0:T(8,128)(2,1)S(1)}, u32[]{:S(2)}, u32[]{:S(2)}) collective-permute-start(bf16[128,3200]{1,0:T(8,128)(2,1)S(1)} %constant_dynamic-update-slice_fusion.6.own_ref), channel_id=1, source_target_pairs={{0,1},{1,0},{2,3},{3,2},{4,5},{5,4},{6,7},{7,6},{8,9},{9,8},{10,11... | collective-permute-start | bytes 2457608 | tf_op jit(solution)/shard_map/ppermute | solution.py:133
  48.0 9.5 %collective-permute-start.18 = (bf16[128,3072]{1,0:T(8,128)(2,1)S(1)}, bf16[128,3072]{1,0:T(8,128)(2,1)S(1)}, u32[]{:S(2)}, u32[]{:S(2)}) collective-permute-start(bf16[128,3072]{1,0:T(8,128)(2,1)S(1)} %get-tuple-element.42), channel_id=1, source_target_pairs={{0,1},{1,0},{2,3},{3,2},{4,5},{5,4},{6,7},{7,6},{8,9},{9,8},{10,11... | collective-permute-start | bytes 2359304 | tf_op jit(solution)/shard_map/ppermute | solution.py:133
  51.3 7.8 %collective-permute-start.3 = (bf16[128,3072]{1,0:T(8,128)(2,1)S(1)}, bf16[128,3072]{1,0:T(8,128)(2,1)S(1)}, u32[]{:S(2)}, u32[]{:S(2)}) collective-permute-start(bf16[128,3072]{1,0:T(8,128)(2,1)S(1)} %get-tuple-element.30), channel_id=1, source_target_pairs={{0,1},{1,0},{2,3},{3,2},{4,5},{5,4},{6,7},{7,6},{8,9},{9,8},{10,11... | collective-permute-start | bytes 2359304 | tf_op jit(solution)/shard_map/ppermute | solution.py:133
  57.4 15.7 %collective-permute-start.26 = (bf16[128,3072]{1,0:T(8,128)(2,1)S(1)}, bf16[128,3072]{1,0:T(8,128)(2,1)S(1)}, u32[]{:S(2)}, u32[]{:S(2)}) collective-permute-start(bf16[128,3072]{1,0:T(8,128)(2,1)S(1)} %get-tuple-element.48), channel_id=1, source_target_pairs={{0,1},{1,0},{2,3},{3,2},{4,5},{5,4},{6,7},{7,6},{8,9},{9,8},{10,11... | collective-permute-start | bytes 2359304 | tf_op jit(solution)/shard_map/ppermute | solution.py:133
  57.7 7.8 %collective-permute-start.19 = (bf16[64,3072]{1,0:T(8,128)(2,1)S(1)}, bf16[64,3072]{1,0:T(8,128)(2,1)S(1)}, u32[]{:S(2)}, u32[]{:S(2)}) collective-permute-start(bf16[64,3072]{1,0:T(8,128)(2,1)S(1)} %get-tuple-element.44), channel_id=1, source_target_pairs={{0,4},{1,3},{2,6},{3,1},{4,0},{5,7},{6,2},{7,5},{8,12},{9,11},{10,... | collective-permute-start | bytes 1179656 | tf_op jit(solution)/shard_map/ppermute | solution.py:133
  59.3 12.3 %collective-permute-start.4 = (bf16[64,3072]{1,0:T(8,128)(2,1)S(1)}, bf16[64,3072]{1,0:T(8,128)(2,1)S(1)}, u32[]{:S(2)}, u32[]{:S(2)}) collective-permute-start(bf16[64,3072]{1,0:T(8,128)(2,1)S(1)} %get-tuple-element.32), channel_id=1, source_target_pairs={{0,4},{1,3},{2,6},{3,1},{4,0},{5,7},{6,2},{7,5},{8,12},{9,11},{10,... | collective-permute-start | bytes 1179656 | tf_op jit(solution)/shard_map/ppermute | solution.py:133
  60.2 18.0 %collective-permute-start.11 = (bf16[64,3072]{1,0:T(8,128)(2,1)S(1)}, bf16[64,3072]{1,0:T(8,128)(2,1)S(1)}, u32[]{:S(2)}, u32[]{:S(2)}) collective-permute-start(bf16[64,3072]{1,0:T(8,128)(2,1)S(1)} %get-tuple-element.38), channel_id=1, source_target_pairs={{0,4},{1,3},{2,6},{3,1},{4,0},{5,7},{6,2},{7,5},{8,12},{9,11},{10,... | collective-permute-start | bytes 1179656 | tf_op jit(solution)/shard_map/ppermute | solution.py:133
  65.6 14.0 %collective-permute-start.20 = (bf16[32,3072]{1,0:T(8,128)(2,1)S(1)}, bf16[32,3072]{1,0:T(8,128)(2,1)S(1)}, u32[]{:S(2)}, u32[]{:S(2)}) collective-permute-start(bf16[32,3072]{1,0:T(8,128)(2,1)S(1)} %get-tuple-element.46), channel_id=1, source_target_pairs={{0,2},{1,5},{2,0},{3,7},{4,6},{5,1},{6,4},{7,3},{8,10},{9,13},{10,... | collective-permute-start | bytes 589832 | tf_op jit(solution)/shard_map/ppermute | solution.py:133
  71.7 21.3 %collective-permute-start.5 = (bf16[32,3072]{1,0:T(8,128)(2,1)S(1)}, bf16[32,3072]{1,0:T(8,128)(2,1)S(1)}, u32[]{:S(2)}, u32[]{:S(2)}) collective-permute-start(bf16[32,3072]{1,0:T(8,128)(2,1)S(1)} %get-tuple-element.34), channel_id=1, source_target_pairs={{0,2},{1,5},{2,0},{3,7},{4,6},{5,1},{6,4},{7,3},{8,10},{9,13},{10,... | collective-permute-start | bytes 589832 | tf_op jit(solution)/shard_map/ppermute | solution.py:133
  73.3 11.2 %collective-permute-start.27 = (bf16[64,3072]{1,0:T(8,128)(2,1)S(1)}, bf16[64,3072]{1,0:T(8,128)(2,1)S(1)}, u32[]{:S(2)}, u32[]{:S(2)}) collective-permute-start(bf16[64,3072]{1,0:T(8,128)(2,1)S(1)} %get-tuple-element.50), channel_id=1, source_target_pairs={{0,4},{1,3},{2,6},{3,1},{4,0},{5,7},{6,2},{7,5},{8,12},{9,11},{10,... | collective-permute-start | bytes 1179656 | tf_op jit(solution)/shard_map/ppermute | solution.py:133
  78.3 7.7 %collective-permute-start.12 = (bf16[32,3072]{1,0:T(8,128)(2,1)S(1)}, bf16[32,3072]{1,0:T(8,128)(2,1)S(1)}, u32[]{:S(2)}, u32[]{:S(2)}) collective-permute-start(bf16[32,3072]{1,0:T(8,128)(2,1)S(1)} %get-tuple-element.40), channel_id=1, source_target_pairs={{0,2},{1,5},{2,0},{3,7},{4,6},{5,1},{6,4},{7,3},{8,10},{9,13},{10,... | collective-permute-start | bytes 589832 | tf_op jit(solution)/shard_map/ppermute | solution.py:133
  79.7 13.3 %collective-permute-start.21 = (bf16[32,3072]{1,0:T(8,128)(2,1)S(1)}, bf16[32,3072]{1,0:T(8,128)(2,1)S(1)}, u32[]{:S(2)}, u32[]{:S(2)}) collective-permute-start(bf16[32,3072]{1,0:T(8,128)(2,1)S(1)} %add_convert_fusion.2), channel_id=1, source_target_pairs={{0,16},{1,17},{2,18},{3,19},{4,20},{5,21},{6,22},{7,23},{8,24},{9,... | collective-permute-start | bytes 589832 | tf_op jit(solution)/shard_map/ppermute | solution.py:133
  86.0 8.5 %collective-permute-start.13 = (bf16[32,3072]{1,0:T(8,128)(2,1)S(1)}, bf16[32,3072]{1,0:T(8,128)(2,1)S(1)}, u32[]{:S(2)}, u32[]{:S(2)}) collective-permute-start(bf16[32,3072]{1,0:T(8,128)(2,1)S(1)} %add_convert_fusion.3), channel_id=1, source_target_pairs={{0,8},{1,9},{2,10},{3,11},{4,12},{5,13},{6,14},{7,15},{8,0},{9,1},... | collective-permute-start | bytes 589832 | tf_op jit(solution)/shard_map/ppermute | solution.py:133
  90.4 7.6 %collective-permute-start.29 = (bf16[32,3072]{1,0:T(8,128)(2,1)S(1)}, bf16[32,3072]{1,0:T(8,128)(2,1)S(1)}, u32[]{:S(2)}, u32[]{:S(2)}) collective-permute-start(bf16[32,3072]{1,0:T(8,128)(2,1)S(1)} %add_convert_fusion.1), channel_id=1, source_target_pairs={{0,24},{1,25},{2,26},{3,27},{4,28},{5,29},{6,30},{7,31},{8,16},{9,... | collective-permute-start | bytes 589832 | tf_op jit(solution)/shard_map/ppermute | solution.py:133
  (14 other events, 73.7 us)

commit v2 on v1

v2 whole, which is shorter than its diff:
```python
import functools

import jax
import jax.numpy as jnp
from jax import lax
from jax.experimental import pallas as pl
from jax.experimental.pallas import tpu as pltpu
from jax.sharding import PartitionSpec as P


GROUPS = 4
eps_norm = 1e-05


VMEM = pl.BlockSpec(memory_space=pltpu.VMEM)
f32 = jnp.float32
bf16 = jnp.bfloat16


def prepare_kernel(n, *refs):
    sources, out_ref, turn_ref, copies, sems = refs[:5], refs[5], refs[6], refs[7:12], refs[12]
    moves = [pltpu.make_async_copy(a, b, sems.at[i]) for i, (a, b) in enumerate(zip(sources, copies))]
    for move in moves:
        move.start()
    for move in moves:
        move.wait()
    tokens_ref, gain_ref, ids_ref, scores_ref, prob_ref = copies
    t, d = tokens_ref.shape
    k = ids_ref.shape[0]
    values = tokens_ref[...].astype(f32)
    average = jnp.mean(values, axis=1, keepdims=True)
    centred = values - average
    variance = jnp.mean(centred * centred, axis=1, keepdims=True)
    normed = centred * lax.rsqrt(variance + eps_norm) * gain_ref[...]
    out_ref[:, :d] = normed.astype(bf16)
    scores = scores_ref[...]
    exp_scores = jnp.exp(scores - jnp.max(scores, axis=0, keepdims=True))
    turn_ref[...] = jnp.zeros(turn_ref.shape, f32)
    turn_ref[:k, :t] = exp_scores / jnp.sum(exp_scores, axis=0, keepdims=True) * prob_ref[...]
    turn_ref[k : 2 * k, :t] = ids_ref[...].astype(f32)
    turned = turn_ref[...].T[:t]
    column = lax.broadcasted_iota(jnp.int32, (t, out_ref.shape[1] - d), 1)
    expert = jnp.where(column >= n, column - n, column).astype(f32)
    value = jnp.zeros(column.shape, f32)
    for j in range(k):
        value = value + jnp.where(expert == turned[:, k + j : k + j + 1], turned[:, j : j + 1], 0.0)
    high = value.astype(bf16).astype(f32)
    low = jnp.where(column < 2 * n, value - high, 0.0)
    out_ref[:, d:] = jnp.where(column < n, high, low).astype(bf16)


def prepare(tokens, norm_gain, expert_ids, expert_scores, group_prob, n):
    t, d = tokens.shape
    width = d + 2 * n + (-2 * n) % 128
    arrays = (tokens, norm_gain[None, :], expert_ids.T, expert_scores.T, group_prob[None, :])
    return pl.pallas_call(
        functools.partial(prepare_kernel, n),
        out_shape=jax.ShapeDtypeStruct((t, width), bf16),
        in_specs=[pl.BlockSpec(memory_space=pltpu.HBM)] * 5,
        out_specs=VMEM,
        scratch_shapes=[pltpu.VMEM((8, 128), f32)]
        + [pltpu.VMEM(a.shape, a.dtype) for a in arrays]
        + [pltpu.SemaphoreType.DMA((5,))],
        compiler_params=pltpu.CompilerParams(vmem_limit_bytes=4 * 2**20),
        name="prepare",
    )(*(pltpu.with_memory_space_constraint(a, pltpu.HBM) for a in arrays))


def expert_kernel(n, own_ref, other_ref, gate_ref, up_ref, down_ref, keep_ref, give_ref, x_ref, h_ref):
    m = own_ref.shape[0]
    d = keep_ref.shape[1]
    x_ref[:m] = own_ref[...]
    x_ref[m:] = other_ref[...]
    me = lax.axis_index("ep")
    columns = x_ref[:, d:].astype(f32)
    index = lax.broadcasted_iota(jnp.int32, columns.shape, 1)
    mine = (index == me) | (index == n + me)
    weight = jnp.sum(jnp.where(mine, columns, 0.0), axis=1, keepdims=True)
    x = x_ref[:, :d]
    gate = jnp.dot(x, gate_ref[0], preferred_element_type=f32)
    up = jnp.dot(x, up_ref[0], preferred_element_type=f32)
    h_ref[...] = (gate * jax.nn.sigmoid(gate) * up).astype(bf16)
    step = 256
    for j in range(0, d, step):
        out = jnp.dot(h_ref[...], down_ref[0, :, j : j + step], preferred_element_type=f32) * weight
        keep_ref[:, j : j + step] = out[:m]
        give_ref[:, j : j + step] = out[m:].astype(bf16)


def expert(own, other, gate_weight, up_weight, down_weight, n):
    m, width = own.shape
    d, ffe = gate_weight.shape[1:]
    block = min(m, 128)
    weights = pl.BlockSpec(memory_space=pltpu.VMEM)
    rows = pl.BlockSpec((block, width), lambda i: (i, 0))
    outs = pl.BlockSpec((block, d), lambda i: (i, 0))
    single = m == block
    return pl.pallas_call(
        functools.partial(expert_kernel, n),
        grid=() if single else (m // block,),
        out_shape=(jax.ShapeDtypeStruct((m, d), f32), jax.ShapeDtypeStruct((m, d), bf16)),
        in_specs=[VMEM if single else rows] * 2 + [weights] * 3,
        out_specs=(VMEM, VMEM) if single else (outs, outs),
        scratch_shapes=[pltpu.VMEM((2 * block, width), bf16), pltpu.VMEM((2 * block, ffe), bf16)],
        compiler_params=pltpu.CompilerParams(vmem_limit_bytes=16 * 2**20),
        cost_estimate=pl.CostEstimate(
            flops=12 * m * d * ffe, bytes_accessed=20 * m * d, transcendentals=2 * m * ffe
        ),
        name="expert",
    )(own, other, gate_weight, up_weight, down_weight)


def join_kernel(low_ref, high_ref, out_ref):
    half = low_ref.shape[0]
    out_ref[:half] = low_ref[...]
    out_ref[half:] = high_ref[...]


def join(low, high):
    m, width = low.shape
    if m > 128:
        return jnp.concatenate([low, high], axis=0)
    return pl.pallas_call(
        join_kernel,
        out_shape=jax.ShapeDtypeStruct((2 * m, width), low.dtype),
        in_specs=[VMEM] * 2,
        out_specs=VMEM,
        compiler_params=pltpu.CompilerParams(vmem_limit_bytes=4 * 2**20),
        cost_estimate=pl.CostEstimate(flops=m * width * 64, bytes_accessed=8 * m * width, transcendentals=0),
        name="join",
    )(low, high)


def merge_kernel(*refs):
    *added, out_ref = refs
    total = added[0][...].astype(f32)
    for ref in added[1:]:
        total = total + ref[...].astype(f32)
    out_ref[...] = total.astype(bf16)


def merge(*arrays):
    m, d = arrays[0].shape
    if m > 256:
        return sum(a.astype(f32) for a in arrays).astype(bf16)
    return pl.pallas_call(
        merge_kernel,
        out_shape=jax.ShapeDtypeStruct((m, d), bf16),
        in_specs=[VMEM] * len(arrays),
        out_specs=VMEM,
        compiler_params=pltpu.CompilerParams(vmem_limit_bytes=4 * 2**20),
        cost_estimate=pl.CostEstimate(flops=m * d * 64, bytes_accessed=10 * m * d, transcendentals=0),
        name="merge",
    )(*arrays)


def fold_kernel(*refs):
    *added, kept_ref, give_ref = refs
    half = kept_ref.shape[0]
    low = added[0][:half].astype(f32)
    high = added[0][half:].astype(f32)
    for ref in added[1:]:
        low = low + ref[:half].astype(f32)
        high = high + ref[half:].astype(f32)
    kept_ref[...] = low
    give_ref[...] = high.astype(bf16)


def fold(*arrays):
    m, d = arrays[0].shape
    half = m // 2
    if m <= 256:
        return pl.pallas_call(
            fold_kernel,
            out_shape=(jax.ShapeDtypeStruct((half, d), f32), jax.ShapeDtypeStruct((half, d), bf16)),
            in_specs=[VMEM] * len(arrays),
            out_specs=(VMEM, VMEM),
            compiler_params=pltpu.CompilerParams(vmem_limit_bytes=4 * 2**20),
            cost_estimate=pl.CostEstimate(flops=m * d * 64, bytes_accessed=12 * m * d, transcendentals=0),
            name="fold",
        )(*arrays)
    total = sum(a.astype(f32) for a in arrays)
    return total[:half], total[half:].astype(bf16)


def local(
    tokens, norm_gain, expert_ids, expert_scores, group_prob, gate_weight, up_weight, down_weight
):
    n = lax.axis_size("ep")
    size = n // GROUPS
    bits = [1 << b for b in range(1, size.bit_length() - 1)]

    def exchange(x, flip):
        return lax.ppermute(x, "ep", [(i, i ^ flip(i)) for i in range(n)])

    def plane(step):
        return lambda i: bits[step] if i % 2 == 0 else bits[-1 - step]

    def group(q):
        return lambda i: q * size

    sent = prepare(tokens, norm_gain, expert_ids, expert_scores, group_prob, n)
    first, rows = {0: sent}, {}
    first[1] = exchange(sent, group(1))
    first[2] = exchange(sent, group(2))
    first[3] = exchange(first[2], group(1))
    for q in range(GROUPS):
        x = first[q]
        for s in range(len(bits)):
            y = exchange(x, plane(s))
            x = join(x, y)
        rows[q] = x
    keep, got = {}, {}
    for q in range(GROUPS):
        other = exchange(rows[q], lambda i: 1)
        keep[q], give = expert(rows[q], other, gate_weight, up_weight, down_weight, n)
        got[q] = exchange(give, lambda i: 1)
    parts = []
    for q in (1, 2, 3, 0):
        kept, extra = keep[q], got[q]
        for s in reversed(range(len(bits))):
            kept, give = fold(kept, extra)
            extra = exchange(give, plane(s))
        if q:
            part = merge(kept, extra)
            parts.append(exchange(part, group(q)))
    return merge(kept, extra, *parts)


def solution(mesh):
    in_specs = (
        P("ep", None), P(), P("ep", None), P("ep", None), P("ep"),
        P("ep", None, None), P("ep", None, None), P("ep", None, None),
    )

    return jax.shard_map(local, mesh=mesh, in_specs=in_specs, out_specs=P("ep", None), check_vma=False)
```

time: 99.1 us -> 103 us (1.039)
  waiting for transfers between devices: 45 us -> 49.1 us
  local copies, waits for them, and re-layouts: 3.88 us -> 0.01 us
  starting transfers between devices: 36.4 us -> 39.1 us
  Pallas kernels: 12.2 us -> 14.1 us
  other arithmetic: 1.13 us -> 0 us
    ppermute x30, waiting for transfers between devices: 45 us -> 49.1 us  [exchange(): return lax.ppermute(x, 'ep', [(i, i ^ flip(i)) for i in range(n)])]
    unnamed x22 -> x6, local copies, waits for them, and re-layouts: 3.77 us -> 0.01 us
    ppermute x30, starting transfers between devices: 36.4 us -> 39.1 us  [exchange(): return lax.ppermute(x, 'ep', [(i, i ^ flip(i)) for i in range(n)])]
    pallas_call x12 -> x24, Pallas kernels: 11.9 us -> 12.8 us  [the longest x4 10.8 us: expert(): pl.pallas_call(functools.partial(expert_kernel, n), grid=() if single els...]
  transfers between devices with their start and end apart: 30 -> 30, of which waited for: 13 -> 13; matrix products, arithmetic and copies ran while one was open for 1% -> 0% of each run, Pallas kernels for 12% -> 12%
where the time goes in v2:
time: 103 us
  waiting for transfers between devices  49.1 us (48%)
  starting transfers between devices  39.1 us (38%)
  Pallas kernels  14.1 us (14%)
    ppermute x30, waiting for transfers between devices, exchange(): return lax.ppermute(x, 'ep', [(i, i ^ flip(i)) for i in range(n)])  49.1 us
    ppermute x30, starting transfers between devices, exchange(): return lax.ppermute(x, 'ep', [(i, i ^ flip(i)) for i in range(n)])  39.1 us
    pallas_call x4, Pallas kernels, expert(): pl.pallas_call(functools.partial(expert_kernel, n), grid=() if single els...  10.8 us
  transfers between devices with their start and end apart: 30, of which 13 were waited for; matrix products, arithmetic and copies ran while one was open for 0% of the time, Pallas kernels for 12%

profile of v2, /device:TPU:0, one launch (start us, length us, event | category | flops | bytes accessed | tf_op | source)
XLA Modules:
  0.0 102.5 jit_solution(14095747540713232747)
XLA Ops:
  1.3 4.1 %collective-permute-start.14 = (bf16[32,3200]{1,0:T(8,128)(2,1)S(1)}, bf16[32,3200]{1,0:T(8,128)(2,1)S(1)}, u32[]{:S(2)}, u32[]{:S(2)}) collective-permute-start(bf16[32,3200]{1,0:T(8,128)(2,1)S(1)} %prepare.1.low_ref), channel_id=1, source_target_pairs={{0,16},{1,17},{2,18},{3,19},{4,20},{5,21},{6,22},{7,23},{8,24},{9,... | collective-permute-start | bytes 614408 | tf_op jit(solution)/shard_map/ppermute | solution.py:194
  7.0 8.0 %collective-permute-done.14.low_ref = bf16[32,3200]{1,0:T(8,128)(2,1)S(1)} collective-permute-done((bf16[32,3200]{1,0:T(8,128)(2,1)S(1)}, bf16[32,3200]{1,0:T(8,128)(2,1)S(1)}, u32[]{:S(2)}, u32[]{:S(2)}) %collective-permute-start.14) | collective-permute-done | bytes 204832 | tf_op jit(solution)/shard_map/ppermute | solution.py:194
  17.7 3.1 %collective-permute-done.15.high_ref = bf16[32,3200]{1,0:T(8,128)(2,1)S(1)} collective-permute-done((bf16[32,3200]{1,0:T(8,128)(2,1)S(1)}, bf16[32,3200]{1,0:T(8,128)(2,1)S(1)}, u32[]{:S(2)}, u32[]{:S(2)}) %collective-permute-start.15) | collective-permute-done | bytes 204832 | tf_op jit(solution)/shard_map/ppermute | solution.py:194
  20.8 1.6 %collective-permute-start.16 = (bf16[64,3200]{1,0:T(8,128)(2,1)S(1)}, bf16[64,3200]{1,0:T(8,128)(2,1)S(1)}, u32[]{:S(2)}, u32[]{:S(2)}) collective-permute-start(bf16[64,3200]{1,0:T(8,128)(2,1)S(1)} %join.12.low_ref), channel_id=1, source_target_pairs={{0,4},{1,3},{2,6},{3,1},{4,0},{5,7},{6,2},{7,5},{8,12},{9,11},{10,... | collective-permute-start | bytes 1228808 | tf_op jit(solution)/shard_map/ppermute | solution.py:194
  24.2 1.9 %collective-permute-start.8 = (bf16[64,3200]{1,0:T(8,128)(2,1)S(1)}, bf16[64,3200]{1,0:T(8,128)(2,1)S(1)}, u32[]{:S(2)}, u32[]{:S(2)}) collective-permute-start(bf16[64,3200]{1,0:T(8,128)(2,1)S(1)} %join.10.low_ref), channel_id=1, source_target_pairs={{0,4},{1,3},{2,6},{3,1},{4,0},{5,7},{6,2},{7,5},{8,12},{9,11},{10,... | collective-permute-start | bytes 1228808 | tf_op jit(solution)/shard_map/ppermute | solution.py:194
  27.5 2.9 %collective-permute-done.23.high_ref = bf16[32,3200]{1,0:T(8,128)(2,1)S(1)} collective-permute-done((bf16[32,3200]{1,0:T(8,128)(2,1)S(1)}, bf16[32,3200]{1,0:T(8,128)(2,1)S(1)}, u32[]{:S(2)}, u32[]{:S(2)}) %collective-permute-start.23) | collective-permute-done | bytes 204832 | tf_op jit(solution)/shard_map/ppermute | solution.py:194
  32.0 2.8 %collective-permute-done.high_ref = bf16[32,3200]{1,0:T(8,128)(2,1)S(1)} collective-permute-done((bf16[32,3200]{1,0:T(8,128)(2,1)S(1)}, bf16[32,3200]{1,0:T(8,128)(2,1)S(1)}, u32[]{:S(2)}, u32[]{:S(2)}) %collective-permute-start) | collective-permute-done | bytes 204832 | tf_op jit(solution)/shard_map/ppermute | solution.py:194
  36.4 4.0 %collective-permute-done.24.high_ref = bf16[64,3200]{1,0:T(8,128)(2,1)S(1)} collective-permute-done((bf16[64,3200]{1,0:T(8,128)(2,1)S(1)}, bf16[64,3200]{1,0:T(8,128)(2,1)S(1)}, u32[]{:S(2)}, u32[]{:S(2)}) %collective-permute-start.24) | collective-permute-done | bytes 409632 | tf_op jit(solution)/shard_map/ppermute | solution.py:194
  40.8 4.1 %collective-permute-done.1.high_ref = bf16[64,3200]{1,0:T(8,128)(2,1)S(1)} collective-permute-done((bf16[64,3200]{1,0:T(8,128)(2,1)S(1)}, bf16[64,3200]{1,0:T(8,128)(2,1)S(1)}, u32[]{:S(2)}, u32[]{:S(2)}) %collective-permute-start.1) | collective-permute-done | bytes 409632 | tf_op jit(solution)/shard_map/ppermute | solution.py:194
  45.1 2.7 %expert.6 = (f32[128,3072]{1,0:T(8,128)S(1)}, bf16[128,3072]{1,0:T(8,128)(2,1)S(1)}) custom-call(bf16[128,3200]{1,0:T(8,128)(2,1)S(1)} %join.13.own_ref, bf16[128,3200]{1,0:T(8,128)(2,1)S(1)} %collective-permute-done.17.other_ref, bf16[1,3072,384]{2,1,0:T(8,128)(2,1)S(1)} %copy-done, bf16[1,3072,384]{2,1,0:T(8,128)(2,1)S(1)} %copy-done.1, ...), custom_call_target="tpu_custom_call" | custom-call | flops 1811939328 | bytes 7864320 | tf_op jit(solution)/shard_map/expert/pallas_call | solution.py:98
  48.3 2.7 %expert.5 = (f32[128,3072]{1,0:T(8,128)S(1)}, bf16[128,3072]{1,0:T(8,128)(2,1)S(1)}) custom-call(bf16[128,3200]{1,0:T(8,128)(2,1)S(1)} %join.11.own_ref, bf16[128,3200]{1,0:T(8,128)(2,1)S(1)} %collective-permute-done.9.other_ref, bf16[1,3072,384]{2,1,0:T(8,128)(2,1)S(1)} %copy-done, bf16[1,3072,384]{2,1,0:T(8,128)(2,1)S(1)} %copy-done.1, ...), custom_call_target="tpu_custom_call" | custom-call | flops 1811939328 | bytes 7864320 | tf_op jit(solution)/shard_map/expert/pallas_call | solution.py:98
  51.2 2.7 %expert.7 = (f32[128,3072]{1,0:T(8,128)S(1)}, bf16[128,3072]{1,0:T(8,128)(2,1)S(1)}) custom-call(bf16[128,3200]{1,0:T(8,128)(2,1)S(1)} %join.15.own_ref, bf16[128,3200]{1,0:T(8,128)(2,1)S(1)} %collective-permute-done.25.other_ref, bf16[1,3072,384]{2,1,0:T(8,128)(2,1)S(1)} %copy-done, bf16[1,3072,384]{2,1,0:T(8,128)(2,1)S(1)} %copy-done.1, ...), custom_call_target="tpu_custom_call" | custom-call | flops 1811939328 | bytes 7864320 | tf_op jit(solution)/shard_map/expert/pallas_call | solution.py:98
  54.3 2.7 %expert.4 = (f32[128,3072]{1,0:T(8,128)S(1)}, bf16[128,3072]{1,0:T(8,128)(2,1)S(1)}) custom-call(bf16[128,3200]{1,0:T(8,128)(2,1)S(1)} %join.9.own_ref, bf16[128,3200]{1,0:T(8,128)(2,1)S(1)} %collective-permute-done.2.other_ref, bf16[1,3072,384]{2,1,0:T(8,128)(2,1)S(1)} %copy-done, bf16[1,3072,384]{2,1,0:T(8,128)(2,1)S(1)} %copy-done.1, ...), custom_call_target="tpu_custom_call" | custom-call | flops 1811939328 | bytes 7864320 | tf_op jit(solution)/shard_map/expert/pallas_call | solution.py:98
  62.1 3.1 %collective-permute-done.19.refs_1_ = bf16[64,3072]{1,0:T(8,128)(2,1)S(1)} collective-permute-done((bf16[64,3072]{1,0:T(8,128)(2,1)S(1)}, bf16[64,3072]{1,0:T(8,128)(2,1)S(1)}, u32[]{:S(2)}, u32[]{:S(2)}) %collective-permute-start.19) | collective-permute-done | bytes 393248 | tf_op jit(solution)/shard_map/ppermute | solution.py:194
  65.3 2.4 %collective-permute-start.20 = (bf16[32,3072]{1,0:T(8,128)(2,1)S(1)}, bf16[32,3072]{1,0:T(8,128)(2,1)S(1)}, u32[]{:S(2)}, u32[]{:S(2)}) collective-permute-start(bf16[32,3072]{1,0:T(8,128)(2,1)S(1)} %get-tuple-element.46), channel_id=1, source_target_pairs={{0,2},{1,5},{2,0},{3,7},{4,6},{5,1},{6,4},{7,3},{8,10},{9,13},{10,... | collective-permute-start | bytes 589832 | tf_op jit(solution)/shard_map/ppermute | solution.py:194
  67.7 2.9 %collective-permute-done.11.refs_1_ = bf16[64,3072]{1,0:T(8,128)(2,1)S(1)} collective-permute-done((bf16[64,3072]{1,0:T(8,128)(2,1)S(1)}, bf16[64,3072]{1,0:T(8,128)(2,1)S(1)}, u32[]{:S(2)}, u32[]{:S(2)}) %collective-permute-start.11) | collective-permute-done | bytes 393248 | tf_op jit(solution)/shard_map/ppermute | solution.py:194
  70.7 3.1 %collective-permute-start.12 = (bf16[32,3072]{1,0:T(8,128)(2,1)S(1)}, bf16[32,3072]{1,0:T(8,128)(2,1)S(1)}, u32[]{:S(2)}, u32[]{:S(2)}) collective-permute-start(bf16[32,3072]{1,0:T(8,128)(2,1)S(1)} %get-tuple-element.40), channel_id=1, source_target_pairs={{0,2},{1,5},{2,0},{3,7},{4,6},{5,1},{6,4},{7,3},{8,10},{9,13},{10,... | collective-permute-start | bytes 589832 | tf_op jit(solution)/shard_map/ppermute | solution.py:194
  73.8 4.1 %collective-permute-done.27.refs_1_ = bf16[64,3072]{1,0:T(8,128)(2,1)S(1)} collective-permute-done((bf16[64,3072]{1,0:T(8,128)(2,1)S(1)}, bf16[64,3072]{1,0:T(8,128)(2,1)S(1)}, u32[]{:S(2)}, u32[]{:S(2)}) %collective-permute-start.27) | collective-permute-done | bytes 393248 | tf_op jit(solution)/shard_map/ppermute | solution.py:194
  77.9 2.4 %collective-permute-start.28 = (bf16[32,3072]{1,0:T(8,128)(2,1)S(1)}, bf16[32,3072]{1,0:T(8,128)(2,1)S(1)}, u32[]{:S(2)}, u32[]{:S(2)}) collective-permute-start(bf16[32,3072]{1,0:T(8,128)(2,1)S(1)} %get-tuple-element.52), channel_id=1, source_target_pairs={{0,2},{1,5},{2,0},{3,7},{4,6},{5,1},{6,4},{7,3},{8,10},{9,13},{10,... | collective-permute-start | bytes 589832 | tf_op jit(solution)/shard_map/ppermute | solution.py:194
  80.3 3.8 %collective-permute-done.4.refs_1_ = bf16[64,3072]{1,0:T(8,128)(2,1)S(1)} collective-permute-done((bf16[64,3072]{1,0:T(8,128)(2,1)S(1)}, bf16[64,3072]{1,0:T(8,128)(2,1)S(1)}, u32[]{:S(2)}, u32[]{:S(2)}) %collective-permute-start.4) | collective-permute-done | bytes 393248 | tf_op jit(solution)/shard_map/ppermute | solution.py:194
  84.2 2.4 %collective-permute-start.5 = (bf16[32,3072]{1,0:T(8,128)(2,1)S(1)}, bf16[32,3072]{1,0:T(8,128)(2,1)S(1)}, u32[]{:S(2)}, u32[]{:S(2)}) collective-permute-start(bf16[32,3072]{1,0:T(8,128)(2,1)S(1)} %get-tuple-element.34), channel_id=1, source_target_pairs={{0,2},{1,5},{2,0},{3,7},{4,6},{5,1},{6,4},{7,3},{8,10},{9,13},{10,... | collective-permute-start | bytes 589832 | tf_op jit(solution)/shard_map/ppermute | solution.py:194
  87.9 3.6 %collective-permute-start.13 = (bf16[32,3072]{1,0:T(8,128)(2,1)S(1)}, bf16[32,3072]{1,0:T(8,128)(2,1)S(1)}, u32[]{:S(2)}, u32[]{:S(2)}) collective-permute-start(bf16[32,3072]{1,0:T(8,128)(2,1)S(1)} %merge.4), channel_id=1, source_target_pairs={{0,8},{1,9},{2,10},{3,11},{4,12},{5,13},{6,14},{7,15},{8,0},{9,1},... | collective-permute-start | bytes 589832 | tf_op jit(solution)/shard_map/ppermute | solution.py:194
  91.6 7.9 %collective-permute-done.21.refs_3_ = bf16[32,3072]{1,0:T(8,128)(2,1)S(1)} collective-permute-done((bf16[32,3072]{1,0:T(8,128)(2,1)S(1)}, bf16[32,3072]{1,0:T(8,128)(2,1)S(1)}, u32[]{:S(2)}, u32[]{:S(2)}) %collective-permute-start.21) | collective-permute-done | bytes 196640 | tf_op jit(solution)/shard_map/ppermute | solution.py:194
  99.5 2.2 %collective-permute-done.29.refs_4_ = bf16[32,3072]{1,0:T(8,128)(2,1)S(1)} collective-permute-done((bf16[32,3072]{1,0:T(8,128)(2,1)S(1)}, bf16[32,3072]{1,0:T(8,128)(2,1)S(1)}, u32[]{:S(2)}, u32[]{:S(2)}) %collective-permute-start.29) | collective-permute-done | bytes 196640 | tf_op jit(solution)/shard_map/ppermute | solution.py:194
  (67 shorter events, 21.0 us)
Async XLA Ops:
  1.3 13.7 %collective-permute-start.14 = (bf16[32,3200]{1,0:T(8,128)(2,1)S(1)}, bf16[32,3200]{1,0:T(8,128)(2,1)S(1)}, u32[]{:S(2)}, u32[]{:S(2)}) collective-permute-start(bf16[32,3200]{1,0:T(8,128)(2,1)S(1)} %prepare.1.low_ref), channel_id=1, source_target_pairs={{0,16},{1,17},{2,18},{3,19},{4,20},{5,21},{6,22},{7,23},{8,24},{9,... | collective-permute-start | bytes 614408 | tf_op jit(solution)/shard_map/ppermute | solution.py:194
  5.5 11.7 %collective-permute-start.6 = (bf16[32,3200]{1,0:T(8,128)(2,1)S(1)}, bf16[32,3200]{1,0:T(8,128)(2,1)S(1)}, u32[]{:S(2)}, u32[]{:S(2)}) collective-permute-start(bf16[32,3200]{1,0:T(8,128)(2,1)S(1)} %prepare.1.low_ref), channel_id=1, source_target_pairs={{0,8},{1,9},{2,10},{3,11},{4,12},{5,13},{6,14},{7,15},{8,0},{9,1},... | collective-permute-start | bytes 614408 | tf_op jit(solution)/shard_map/ppermute | solution.py:194
  20.8 11.1 %collective-permute-start.16 = (bf16[64,3200]{1,0:T(8,128)(2,1)S(1)}, bf16[64,3200]{1,0:T(8,128)(2,1)S(1)}, u32[]{:S(2)}, u32[]{:S(2)}) collective-permute-start(bf16[64,3200]{1,0:T(8,128)(2,1)S(1)} %join.12.low_ref), channel_id=1, source_target_pairs={{0,4},{1,3},{2,6},{3,1},{4,0},{5,7},{6,2},{7,5},{8,12},{9,11},{10,... | collective-permute-start | bytes 1228808 | tf_op jit(solution)/shard_map/ppermute | solution.py:194
  22.4 8.0 %collective-permute-start.23 = (bf16[32,3200]{1,0:T(8,128)(2,1)S(1)}, bf16[32,3200]{1,0:T(8,128)(2,1)S(1)}, u32[]{:S(2)}, u32[]{:S(2)}) collective-permute-start(bf16[32,3200]{1,0:T(8,128)(2,1)S(1)} %collective-permute-done.22.low_ref), channel_id=1, source_target_pairs={{0,2},{1,5},{2,0},{3,7},{4,6},{5,1},{6,4},{7,3},{8,10},{9,13},{10,... | collective-permute-start | bytes 614408 | tf_op jit(solution)/shard_map/ppermute | solution.py:194
  24.2 12.1 %collective-permute-start.8 = (bf16[64,3200]{1,0:T(8,128)(2,1)S(1)}, bf16[64,3200]{1,0:T(8,128)(2,1)S(1)}, u32[]{:S(2)}, u32[]{:S(2)}) collective-permute-start(bf16[64,3200]{1,0:T(8,128)(2,1)S(1)} %join.10.low_ref), channel_id=1, source_target_pairs={{0,4},{1,3},{2,6},{3,1},{4,0},{5,7},{6,2},{7,5},{8,12},{9,11},{10,... | collective-permute-start | bytes 1228808 | tf_op jit(solution)/shard_map/ppermute | solution.py:194
  26.0 8.7 %collective-permute-start = (bf16[32,3200]{1,0:T(8,128)(2,1)S(1)}, bf16[32,3200]{1,0:T(8,128)(2,1)S(1)}, u32[]{:S(2)}, u32[]{:S(2)}) collective-permute-start(bf16[32,3200]{1,0:T(8,128)(2,1)S(1)} %prepare.1.low_ref), channel_id=1, source_target_pairs={{0,2},{1,5},{2,0},{3,7},{4,6},{5,1},{6,4},{7,3},{8,10},{9,13},{10,... | collective-permute-start | bytes 614408 | tf_op jit(solution)/shard_map/ppermute | solution.py:194
  30.4 10.0 %collective-permute-start.24 = (bf16[64,3200]{1,0:T(8,128)(2,1)S(1)}, bf16[64,3200]{1,0:T(8,128)(2,1)S(1)}, u32[]{:S(2)}, u32[]{:S(2)}) collective-permute-start(bf16[64,3200]{1,0:T(8,128)(2,1)S(1)} %join.14.low_ref), channel_id=1, source_target_pairs={{0,4},{1,3},{2,6},{3,1},{4,0},{5,7},{6,2},{7,5},{8,12},{9,11},{10,... | collective-permute-start | bytes 1228808 | tf_op jit(solution)/shard_map/ppermute | solution.py:194
  32.0 13.1 %collective-permute-start.17 = (bf16[128,3200]{1,0:T(8,128)(2,1)S(1)}, bf16[128,3200]{1,0:T(8,128)(2,1)S(1)}, u32[]{:S(2)}, u32[]{:S(2)}) collective-permute-start(bf16[128,3200]{1,0:T(8,128)(2,1)S(1)} %join.13.own_ref), channel_id=1, source_target_pairs={{0,1},{1,0},{2,3},{3,2},{4,5},{5,4},{6,7},{7,6},{8,9},{9,8},{10,11... | collective-permute-start | bytes 2457608 | tf_op jit(solution)/shard_map/ppermute | solution.py:194
  34.8 10.0 %collective-permute-start.1 = (bf16[64,3200]{1,0:T(8,128)(2,1)S(1)}, bf16[64,3200]{1,0:T(8,128)(2,1)S(1)}, u32[]{:S(2)}, u32[]{:S(2)}) collective-permute-start(bf16[64,3200]{1,0:T(8,128)(2,1)S(1)} %join.8.low_ref), channel_id=1, source_target_pairs={{0,4},{1,3},{2,6},{3,1},{4,0},{5,7},{6,2},{7,5},{8,12},{9,11},{10,... | collective-permute-start | bytes 1228808 | tf_op jit(solution)/shard_map/ppermute | solution.py:194
  36.4 11.9 %collective-permute-start.9 = (bf16[128,3200]{1,0:T(8,128)(2,1)S(1)}, bf16[128,3200]{1,0:T(8,128)(2,1)S(1)}, u32[]{:S(2)}, u32[]{:S(2)}) collective-permute-start(bf16[128,3200]{1,0:T(8,128)(2,1)S(1)} %join.11.own_ref), channel_id=1, source_target_pairs={{0,1},{1,0},{2,3},{3,2},{4,5},{5,4},{6,7},{7,6},{8,9},{9,8},{10,11... | collective-permute-start | bytes 2457608 | tf_op jit(solution)/shard_map/ppermute | solution.py:194
  40.5 10.6 %collective-permute-start.25 = (bf16[128,3200]{1,0:T(8,128)(2,1)S(1)}, bf16[128,3200]{1,0:T(8,128)(2,1)S(1)}, u32[]{:S(2)}, u32[]{:S(2)}) collective-permute-start(bf16[128,3200]{1,0:T(8,128)(2,1)S(1)} %join.15.own_ref), channel_id=1, source_target_pairs={{0,1},{1,0},{2,3},{3,2},{4,5},{5,4},{6,7},{7,6},{8,9},{9,8},{10,11... | collective-permute-start | bytes 2457608 | tf_op jit(solution)/shard_map/ppermute | solution.py:194
  44.9 9.4 %collective-permute-start.2 = (bf16[128,3200]{1,0:T(8,128)(2,1)S(1)}, bf16[128,3200]{1,0:T(8,128)(2,1)S(1)}, u32[]{:S(2)}, u32[]{:S(2)}) collective-permute-start(bf16[128,3200]{1,0:T(8,128)(2,1)S(1)} %join.9.own_ref), channel_id=1, source_target_pairs={{0,1},{1,0},{2,3},{3,2},{4,5},{5,4},{6,7},{7,6},{8,9},{9,8},{10,11... | collective-permute-start | bytes 2457608 | tf_op jit(solution)/shard_map/ppermute | solution.py:194
  47.8 9.4 %collective-permute-start.18 = (bf16[128,3072]{1,0:T(8,128)(2,1)S(1)}, bf16[128,3072]{1,0:T(8,128)(2,1)S(1)}, u32[]{:S(2)}, u32[]{:S(2)}) collective-permute-start(bf16[128,3072]{1,0:T(8,128)(2,1)S(1)} %get-tuple-element.42), channel_id=1, source_target_pairs={{0,1},{1,0},{2,3},{3,2},{4,5},{5,4},{6,7},{7,6},{8,9},{9,8},{10,11... | collective-permute-start | bytes 2359304 | tf_op jit(solution)/shard_map/ppermute | solution.py:194
  51.0 7.9 %collective-permute-start.10 = (bf16[128,3072]{1,0:T(8,128)(2,1)S(1)}, bf16[128,3072]{1,0:T(8,128)(2,1)S(1)}, u32[]{:S(2)}, u32[]{:S(2)}) collective-permute-start(bf16[128,3072]{1,0:T(8,128)(2,1)S(1)} %get-tuple-element.36), channel_id=1, source_target_pairs={{0,1},{1,0},{2,3},{3,2},{4,5},{5,4},{6,7},{7,6},{8,9},{9,8},{10,11... | collective-permute-start | bytes 2359304 | tf_op jit(solution)/shard_map/ppermute | solution.py:194
  57.4 7.8 %collective-permute-start.19 = (bf16[64,3072]{1,0:T(8,128)(2,1)S(1)}, bf16[64,3072]{1,0:T(8,128)(2,1)S(1)}, u32[]{:S(2)}, u32[]{:S(2)}) collective-permute-start(bf16[64,3072]{1,0:T(8,128)(2,1)S(1)} %get-tuple-element.44), channel_id=1, source_target_pairs={{0,4},{1,3},{2,6},{3,1},{4,0},{5,7},{6,2},{7,5},{8,12},{9,11},{10,... | collective-permute-start | bytes 1179656 | tf_op jit(solution)/shard_map/ppermute | solution.py:194
  59.0 11.6 %collective-permute-start.11 = (bf16[64,3072]{1,0:T(8,128)(2,1)S(1)}, bf16[64,3072]{1,0:T(8,128)(2,1)S(1)}, u32[]{:S(2)}, u32[]{:S(2)}) collective-permute-start(bf16[64,3072]{1,0:T(8,128)(2,1)S(1)} %get-tuple-element.38), channel_id=1, source_target_pairs={{0,4},{1,3},{2,6},{3,1},{4,0},{5,7},{6,2},{7,5},{8,12},{9,11},{10,... | collective-permute-start | bytes 1179656 | tf_op jit(solution)/shard_map/ppermute | solution.py:194
  59.8 18.0 %collective-permute-start.27 = (bf16[64,3072]{1,0:T(8,128)(2,1)S(1)}, bf16[64,3072]{1,0:T(8,128)(2,1)S(1)}, u32[]{:S(2)}, u32[]{:S(2)}) collective-permute-start(bf16[64,3072]{1,0:T(8,128)(2,1)S(1)} %get-tuple-element.50), channel_id=1, source_target_pairs={{0,4},{1,3},{2,6},{3,1},{4,0},{5,7},{6,2},{7,5},{8,12},{9,11},{10,... | collective-permute-start | bytes 1179656 | tf_op jit(solution)/shard_map/ppermute | solution.py:194
  61.4 22.7 %collective-permute-start.4 = (bf16[64,3072]{1,0:T(8,128)(2,1)S(1)}, bf16[64,3072]{1,0:T(8,128)(2,1)S(1)}, u32[]{:S(2)}, u32[]{:S(2)}) collective-permute-start(bf16[64,3072]{1,0:T(8,128)(2,1)S(1)} %get-tuple-element.32), channel_id=1, source_target_pairs={{0,4},{1,3},{2,6},{3,1},{4,0},{5,7},{6,2},{7,5},{8,12},{9,11},{10,... | collective-permute-start | bytes 1179656 | tf_op jit(solution)/shard_map/ppermute | solution.py:194
  65.3 21.4 %collective-permute-start.20 = (bf16[32,3072]{1,0:T(8,128)(2,1)S(1)}, bf16[32,3072]{1,0:T(8,128)(2,1)S(1)}, u32[]{:S(2)}, u32[]{:S(2)}) collective-permute-start(bf16[32,3072]{1,0:T(8,128)(2,1)S(1)} %get-tuple-element.46), channel_id=1, source_target_pairs={{0,2},{1,5},{2,0},{3,7},{4,6},{5,1},{6,4},{7,3},{8,10},{9,13},{10,... | collective-permute-start | bytes 589832 | tf_op jit(solution)/shard_map/ppermute | solution.py:194
  70.7 17.1 %collective-permute-start.12 = (bf16[32,3072]{1,0:T(8,128)(2,1)S(1)}, bf16[32,3072]{1,0:T(8,128)(2,1)S(1)}, u32[]{:S(2)}, u32[]{:S(2)}) collective-permute-start(bf16[32,3072]{1,0:T(8,128)(2,1)S(1)} %get-tuple-element.40), channel_id=1, source_target_pairs={{0,2},{1,5},{2,0},{3,7},{4,6},{5,1},{6,4},{7,3},{8,10},{9,13},{10,... | collective-permute-start | bytes 589832 | tf_op jit(solution)/shard_map/ppermute | solution.py:194
  77.9 13.6 %collective-permute-start.28 = (bf16[32,3072]{1,0:T(8,128)(2,1)S(1)}, bf16[32,3072]{1,0:T(8,128)(2,1)S(1)}, u32[]{:S(2)}, u32[]{:S(2)}) collective-permute-start(bf16[32,3072]{1,0:T(8,128)(2,1)S(1)} %get-tuple-element.52), channel_id=1, source_target_pairs={{0,2},{1,5},{2,0},{3,7},{4,6},{5,1},{6,4},{7,3},{8,10},{9,13},{10,... | collective-permute-start | bytes 589832 | tf_op jit(solution)/shard_map/ppermute | solution.py:194
  86.7 12.8 %collective-permute-start.21 = (bf16[32,3072]{1,0:T(8,128)(2,1)S(1)}, bf16[32,3072]{1,0:T(8,128)(2,1)S(1)}, u32[]{:S(2)}, u32[]{:S(2)}) collective-permute-start(bf16[32,3072]{1,0:T(8,128)(2,1)S(1)} %merge.5), channel_id=1, source_target_pairs={{0,16},{1,17},{2,18},{3,19},{4,20},{5,21},{6,22},{7,23},{8,24},{9,... | collective-permute-start | bytes 589832 | tf_op jit(solution)/shard_map/ppermute | solution.py:194
  87.9 11.6 %collective-permute-start.13 = (bf16[32,3072]{1,0:T(8,128)(2,1)S(1)}, bf16[32,3072]{1,0:T(8,128)(2,1)S(1)}, u32[]{:S(2)}, u32[]{:S(2)}) collective-permute-start(bf16[32,3072]{1,0:T(8,128)(2,1)S(1)} %merge.4), channel_id=1, source_target_pairs={{0,8},{1,9},{2,10},{3,11},{4,12},{5,13},{6,14},{7,15},{8,0},{9,1},... | collective-permute-start | bytes 589832 | tf_op jit(solution)/shard_map/ppermute | solution.py:194
  91.5 10.2 %collective-permute-start.29 = (bf16[32,3072]{1,0:T(8,128)(2,1)S(1)}, bf16[32,3072]{1,0:T(8,128)(2,1)S(1)}, u32[]{:S(2)}, u32[]{:S(2)}) collective-permute-start(bf16[32,3072]{1,0:T(8,128)(2,1)S(1)} %merge.6), channel_id=1, source_target_pairs={{0,24},{1,25},{2,26},{3,27},{4,28},{5,29},{6,30},{7,31},{8,16},{9,... | collective-permute-start | bytes 589832 | tf_op jit(solution)/shard_map/ppermute | solution.py:194
  (9 other events, 66.8 us)
